TPU v7x, 32 devices: a whole 2x2x4 slice. The times are simulated.
32 devices in a mesh: kv: 16 (over z, x, core), tp: 2 (over y).
Axes of the slice: x: 2, y: 2, z: 4, core: 2. Of those that a mesh axis runs over, the one named last changes fastest.
Arguments:
- queries: bfloat16 [2048, 4096], P('kv', 'tp'), may hold values from -6 to 6
- keys: bfloat16 [2048, 512], P('kv', 'tp'), may hold values from -6 to 6
- values: bfloat16 [2048, 512], P('kv', 'tp'), may hold values from -6 to 6
- logsum: float32 [2048, 32], P('kv', 'tp'), may hold values from 2 to 6
- out_grad: bfloat16 [2048, 4096], P('kv', 'tp'), may hold values from -6 to 6
- normed_input: bfloat16 [2048, 4096], P('kv', 'tp'), may hold values from -6 to 6
- chosen: int32 [32, 16], P('kv'), may hold values from 0 to 63, as said below
Outputs:
- query_grad: float32 [2048, 4096], P('kv', 'tp')
- key_grad: float32 [2048, 512], P('kv', 'tp')
- value_grad: float32 [2048, 512], P('kv', 'tp')
- value_weight_grad: float32 [4096, 512], P('kv', 'tp')
Inputs may be any that keep to these rules, and one draw needn't show every extreme that they name: `chosen`: each row r names 16 distinct key blocks, among them block 0 and the blocks r * 2 to r * 2 + 64 / 32 - 1 that hold the query block's own positions. The rows of one device (aligned runs of 2 rows) name at most one block of any other device's 128 / 32 blocks. Blocks after the query block may be named; their keys are masked.
All inputs are finite; a program needn't handle non-finite values.
Results may differ from a plain program's by a relative error of at most 0.008.
Values may be sent and summed in bfloat16 or wider, within the bound.
A program may use at most 64 MiB of HBM per device.

v0:
```python
import jax
import jax.numpy as jnp
from jax import lax
from jax.sharding import PartitionSpec as P

HD = 128
QB = 64
KB = 32
NSEL = 16


def local(queries, keys, values, logsum, out_grad, normed_input, chosen):
    devices = lax.axis_size("kv")
    here = lax.axis_index("kv")
    tok = keys.shape[0]
    kv_cols = keys.shape[1]
    kv_heads = kv_cols // HD
    group = queries.shape[1] // kv_cols
    kblocks = tok // KB
    qblocks = tok // QB
    span = NSEL * KB
    scale = HD ** (-0.5)
    owner = chosen // kblocks
    within = chosen % kblocks
    remote = owner != here
    peers = jnp.arange(devices, dtype=jnp.int32)
    named = (owner[:, :, None] == peers[None, None, :]) & remote[:, :, None]
    wanted = jnp.max(jnp.where(named, within[:, :, None] + 1, 0), axis=(0, 1))
    asked = (
        lax.all_to_all(
            wanted.reshape(devices, 1), "kv", split_axis=0, concat_axis=0, tiled=True
        ).reshape(devices)
        - 1
    )
    key_blocks = keys.reshape(kblocks, KB, kv_cols)
    value_blocks = values.reshape(kblocks, KB, kv_cols)
    taken = jnp.maximum(asked, 0)
    live = (asked >= 0)[:, None, None]
    send_keys = jnp.where(live, key_blocks[taken], jnp.zeros((), keys.dtype))
    send_values = jnp.where(live, value_blocks[taken], jnp.zeros((), values.dtype))
    got_keys, got_values = (
        lax.all_to_all(send_keys, "kv", split_axis=0, concat_axis=0, tiled=True),
        lax.all_to_all(send_values, "kv", split_axis=0, concat_axis=0, tiled=True),
    )
    pool_keys = jnp.concatenate([key_blocks, got_keys], axis=0)
    pool_values = jnp.concatenate([value_blocks, got_values], axis=0)
    slot = jnp.where(remote, kblocks + owner, within)
    sel_keys = pool_keys[slot].reshape(qblocks, span, kv_heads, HD)
    sel_values = pool_values[slot].reshape(qblocks, span, kv_heads, HD)
    query_rows = queries.reshape(qblocks, QB, kv_heads, group, HD)
    dout = out_grad.reshape(qblocks, QB, kv_heads, group, HD)
    lse = logsum.reshape(qblocks, QB, kv_heads, group)
    scores = (
        jnp.einsum("bqngd,bjnd->bqngj", query_rows, sel_keys, preferred_element_type=jnp.float32)
        * scale
    )
    qpos = here * tok + jnp.arange(tok, dtype=jnp.int32).reshape(qblocks, QB)
    kpos = (chosen[:, :, None] * KB + jnp.arange(KB, dtype=jnp.int32)[None, None, :]).reshape(
        qblocks, span
    )
    valid = (kpos[:, None, :] <= qpos[:, :, None])[:, :, None, None, :]
    prob = jnp.where(valid, jnp.exp(scores - lse[..., None]), 0.0)
    dprob = jnp.einsum("bqngd,bjnd->bqngj", dout, sel_values, preferred_element_type=jnp.float32)
    delta = jnp.sum(prob * dprob, axis=-1, keepdims=True)
    dscore = (prob * (dprob - delta)).astype(jnp.bfloat16)
    prob_low = prob.astype(jnp.bfloat16)
    query_grad = (
        jnp.einsum("bqngj,bjnd->bqngd", dscore, sel_keys, preferred_element_type=jnp.float32)
        * scale
    )
    query_grad = query_grad.reshape(tok, queries.shape[1])
    key_part = (
        jnp.einsum("bqngj,bqngd->bjnd", dscore, query_rows, preferred_element_type=jnp.float32)
        * scale
    )
    value_part = jnp.einsum("bqngj,bqngd->bjnd", prob_low, dout, preferred_element_type=jnp.float32)
    entries = qblocks * NSEL
    pool_size = kblocks + devices
    onehot = (slot.reshape(entries, 1) == jnp.arange(pool_size, dtype=jnp.int32)[None, :]).astype(
        jnp.float32
    )
    key_sum = jnp.dot(
        onehot.T,
        key_part.reshape(entries, KB * kv_cols),
        precision=lax.Precision.HIGHEST,
        preferred_element_type=jnp.float32,
    )
    value_sum = jnp.dot(
        onehot.T,
        value_part.reshape(entries, KB * kv_cols),
        precision=lax.Precision.HIGHEST,
        preferred_element_type=jnp.float32,
    )
    back_keys = key_sum[kblocks:].reshape(devices, KB, kv_cols)
    back_values = value_sum[kblocks:].reshape(devices, KB, kv_cols)
    ret_keys, ret_values = (
        lax.all_to_all(back_keys, "kv", split_axis=0, concat_axis=0, tiled=True),
        lax.all_to_all(back_values, "kv", split_axis=0, concat_axis=0, tiled=True),
    )
    home = (asked[:, None] == jnp.arange(kblocks, dtype=jnp.int32)[None, :]).astype(jnp.float32)
    key_grad = key_sum[:kblocks] + jnp.dot(
        home.T,
        ret_keys.reshape(devices, KB * kv_cols),
        precision=lax.Precision.HIGHEST,
        preferred_element_type=jnp.float32,
    )
    value_grad = value_sum[:kblocks] + jnp.dot(
        home.T,
        ret_values.reshape(devices, KB * kv_cols),
        precision=lax.Precision.HIGHEST,
        preferred_element_type=jnp.float32,
    )
    key_grad = key_grad.reshape(tok, kv_cols)
    value_grad = value_grad.reshape(tok, kv_cols)
    value_low = value_grad.astype(jnp.bfloat16)
    full_input = lax.all_gather(normed_input, "tp", axis=1, tiled=True)
    weight_grad = lax.psum_scatter(
        jnp.einsum("td,tc->dc", full_input, value_low, preferred_element_type=jnp.float32),
        "kv",
        scatter_dimension=0,
        tiled=True,
    )
    return (query_grad, key_grad, value_grad, weight_grad)


def solution(mesh):
    in_specs = (
        P("kv", "tp"),
        P("kv", "tp"),
        P("kv", "tp"),
        P("kv", "tp"),
        P("kv", "tp"),
        P("kv", "tp"),
        P("kv", None),
    )
    out_specs = (P("kv", "tp"), P("kv", "tp"), P("kv", "tp"), P("kv", "tp"))
    return jax.shard_map(local, mesh=mesh, in_specs=in_specs, out_specs=out_specs, check_vma=False)
```

profile of v0, /device:TPU:0, one launch (start us, length us, event | category | flops | bytes accessed | tf_op | source)
XLA Modules:
  0.0 171.1 jit_solution(7793433736477169849)
XLA Ops:
  7.2 0.8 compare_select_fusion
  8.1 0.7 copy.55
  8.7 7.4 %all-to-all-start = ((s32[16,1,1]{2,1,0:T(1,128)}), s32[16,1,1]{2,1,0:T(1,128)S(1)}, u32[]{:S(2)}, u32[]{:S(2)}) async-start(s32[16,1,1]{2,1,0:T(1,128)} %copy.55), calls=%async_computation | async-start | bytes 16384 | tf_op jit(solution)/shard_map/all_to_all | solution.py:30
  16.2 6.3 %all-to-all-done = s32[16,1,1]{2,1,0:T(1,128)S(1)} async-done(((s32[16,1,1]{2,1,0:T(1,128)}), s32[16,1,1]{2,1,0:T(1,128)S(1)}, u32[]{:S(2)}, u32[]{:S(2)}) %all-to-all-start) | async-done | bytes 96 | tf_op jit(solution)/shard_map/all_to_all | solution.py:30
  22.5 0.7 fusion.35
  23.2 1.4 gather_fusion.2
  24.6 1.4 gather_fusion
  26.0 0.4 compare_reduce_fusion
  26.4 0.8 broadcast_select_fusion.1
  27.2 3.5 %all-to-all-start.1 = ((bf16[16,32,256]{2,1,0:T(8,128)(2,1)}), bf16[16,32,256]{2,1,0:T(8,128)(2,1)S(1)}, u32[]{:S(2)}, u32[]{:S(2)}) async-start(bf16[16,32,256]{2,1,0:T(8,128)(2,1)} %get-tuple-element.31), calls=%async_computation.1 | async-start | bytes 524288 | tf_op jit(solution)/shard_map/all_to_all | solution.py:42
  31.1 0.8 sub.31
  31.9 1.1 copy.79
  33.3 7.4 %all-to-all-done.1 = bf16[16,32,256]{2,1,0:T(8,128)(2,1)S(1)} async-done(((bf16[16,32,256]{2,1,0:T(8,128)(2,1)}), bf16[16,32,256]{2,1,0:T(8,128)(2,1)S(1)}, u32[]{:S(2)}, u32[]{:S(2)}) %all-to-all-start.1) | async-done | bytes 262176 | tf_op jit(solution)/shard_map/all_to_all | solution.py:42
  40.8 0.6 gather_fusion.1
  41.5 0.7 fusion.20
  42.2 2.0 %copy-done = f32[2,2,512,64,8]{2,3,4,1,0:T(8,128)} copy-done((f32[2,2,512,64,8]{2,3,4,1,0:T(8,128)}, f32[2,2,512,64,8]{2,3,4,1,0:T(8,128)S(1)}, u32[]{:S(2)}) %copy-start) | copy-done | bytes 4194328
  44.2 1.8 %fusion.14 = f32[2,512,2,128]{3,1,2,0:T(8,128)S(1)} fusion(f32[2,2,512,64,8]{2,3,4,1,0:T(8,128)S(1)} %fusion.20, f32[2,64,2,8]{1,3,2,0:T(8,128)S(1)} %copy.58, pred[2,64,512]{2,1,0:T(8,128)(4,1)S(1)} %broadcast_compare_fusion, bf16[2,64,2,8,128]{4,3,2,1,0:T(8,128)(2,1)S(1)} %bitcast.77), kind=kOutput, calls=%fused_computation.24 | convolution fusion | flops 272629760 | bytes 5840896 | tf_op jit(solution)/shard_map/bqngj,bqngd->bjnd/dot_general | solution.py:76
  46.0 0.8 copy.66
  46.8 0.8 reshape.135
  47.6 0.6 fusion.28
  48.3 1.0 copy.83
  49.3 3.6 %all-to-all-start.4 = ((f32[16,32,256]{2,1,0:T(8,128)}), f32[16,32,256]{2,1,0:T(8,128)S(1)}, u32[]{:S(2)}, u32[]{:S(2)}) async-start(f32[16,32,256]{2,1,0:T(8,128)} %bitcast.30), calls=%async_computation.4 | async-start | bytes 1048576 | tf_op jit(solution)/shard_map/all_to_all | solution.py:98
  52.9 0.7 all-gather.2.cloned.1.call-update
  53.6 13.5 %all-to-all-done.4 = f32[16,32,256]{2,1,0:T(8,128)S(1)} async-done(((f32[16,32,256]{2,1,0:T(8,128)}), f32[16,32,256]{2,1,0:T(8,128)S(1)}, u32[]{:S(2)}, u32[]{:S(2)}) %all-to-all-start.4) | async-done | bytes 524320 | tf_op jit(solution)/shard_map/all_to_all | solution.py:98
  67.1 0.3 copy.84
  67.4 0.4 convolution_add_fusion
  67.9 9.9 %all-gather.2.cloned.1.call-done = bf16[128,4096]{1,0:T(8,128)(2,1)} async-done(((bf16[128,2048]{1,0:T(8,128)(2,1)}), bf16[128,4096]{1,0:T(8,128)(2,1)}) %all-gather.2.cloned.1.call-update) | async-done | bytes 1048592 | tf_op jit(solution)/shard_map/all_gather | solution.py:116
  77.8 3.9 %convolution_bitcast_fusion = f32[4096,256]{0,1:T(8,128)} fusion(bf16[128,4096]{1,0:T(8,128)(2,1)} %all-gather.2.cloned.1.call-done, f32[128,256]{1,0:T(8,128)S(1)} %reshape.138), kind=kOutput, calls=%fused_computation.6 | convolution fusion | flops 268468224 | bytes 5373952 | tf_op jit(solution)/shard_map/td,tc->dc/dot_general | solution.py:118
  81.7 15.6 %all_to_all.29 = bf16[16,32,256]{2,1,0:T(8,128)(2,1)S(1)} all-to-all(bf16[16,32,256]{2,1,0:T(8,128)(2,1)S(1)} %get-tuple-element.32), channel_id=1, replica_groups=mesh['kv'=16,'tp'=2] {'kv'}, dimensions={0} | all-to-all | bytes 524288 | tf_op jit(solution)/shard_map/all_to_all | solution.py:43
  97.3 0.6 gather_fusion.3
  98.1 3.6 %fusion = (f32[2,64,2,8]{1,3,2,0:T(8,128)S(1)}, f32[2,2,512,64,8]{2,3,4,1,0:T(8,128)S(1)}) fusion(f32[2,2,512,64,8]{2,3,4,1,0:T(8,128)} %copy-done, f32[2,64,2,8]{1,3,2,0:T(8,128)S(1)} %copy.58, pred[2,64,512]{2,1,0:T(8,128)(4,1)S(1)} %broadcast_compare_fusion, bf16[2,64,2,8,128]{4,3,2,1,0:T(8,128)(2,1)S(1)} %bitcast.78, ...), kind=kOutput, calls=%fused_computation.9 | convolution fusion | flops 273676288 | bytes 9519104 | tf_op jit(solution)/shard_map/bqngd,bjnd->bqngj/dot_general | solution.py:63
  101.7 0.3 copy-done.1
  101.9 1.5 fusion.2
  103.5 0.9 fusion.13
  104.4 1.8 %copy.64 = f32[2,512,2,128]{3,2,1,0:T(2,128)} copy(f32[2,512,2,128]{3,1,2,0:T(8,128)S(1)} %fusion.13) | data formatting | bytes 2097152 | tf_op jit(solution)/shard_map/mul | solution.py:73
  106.2 3.0 %reshape.131 = f32[32,8192]{1,0:T(8,128)} reshape(f32[2,512,2,128]{3,2,1,0:T(2,128)} %copy.64) | data formatting | bytes 2097152 | tf_op jit(solution)/shard_map/reshape | solution.py:84
  109.2 1.8 %fusion.29 = f32[20,8192]{1,0:T(8,128)S(1)} fusion(f32[32,8192]{1,0:T(8,128)} %reshape.131, s32[32]{0:T(128)S(1)} %eq.46), kind=kOutput, calls=%fused_computation.45 | convolution fusion | flops 62915200 | bytes 1704064 | tf_op jit(solution)/shard_map/dot_general | solution.py:82
  111.1 1.0 copy.81
  112.0 4.2 %all-to-all-start.3 = ((f32[16,32,256]{2,1,0:T(8,128)}), f32[16,32,256]{2,1,0:T(8,128)}, u32[]{:S(2)}, u32[]{:S(2)}) async-start(f32[16,32,256]{2,1,0:T(8,128)} %bitcast.81), calls=%async_computation.3 | async-start | bytes 1048576 | tf_op jit(solution)/shard_map/all_to_all | solution.py:97
  116.3 0.7 fusion.17
  117.0 0.6 copy.62
  117.6 1.1 reshape.130
  118.8 17.0 %all-to-all-done.3 = f32[16,32,256]{2,1,0:T(8,128)} async-done(((f32[16,32,256]{2,1,0:T(8,128)}), f32[16,32,256]{2,1,0:T(8,128)}, u32[]{:S(2)}, u32[]{:S(2)}) %all-to-all-start.3) | async-done | bytes 524320 | tf_op jit(solution)/shard_map/all_to_all | solution.py:97
  135.8 1.4 copy.82
  137.1 0.4 convolution_add_fusion.1
  137.5 0.7 reshape.134
  138.3 24.2 %reduce-scatter.2.cloned.1.call-done = f32[256,256]{0,1:T(8,128)} async-done(((f32[4096,256]{0,1:T(8,128)}), f32[256,256]{0,1:T(8,128)}) %reduce-scatter.2.cloned.1.call-update) | async-done | bytes 262160 | tf_op jit(solution)/shard_map/reduce_scatter | solution.py:117
  162.4 1.8 %copy.67 = f32[256,256]{1,0:T(8,128)} copy(f32[256,256]{0,1:T(8,128)} %reduce-scatter.2.cloned.1.call-done) | data formatting | bytes 524288
  (39 shorter events, 1.4 us)
Async XLA Ops:
  7.2 33.6 %copy-start.4 = (bf16[128,256]{1,0:T(8,128)(2,1)S(1)}, bf16[128,256]{1,0:T(8,128)(2,1)}, u32[]{:S(2)}) copy-start(bf16[128,256]{1,0:T(8,128)(2,1)} %param.8) | copy-start | bytes 196612
  7.2 25.8 %copy-start.6 = (bf16[128,2048]{1,0:T(8,128)(2,1)S(1)}, bf16[128,2048]{1,0:T(8,128)(2,1)}, u32[]{:S(2)}) copy-start(bf16[128,2048]{1,0:T(8,128)(2,1)} %param.11) | copy-start | bytes 1572868
  8.7 13.8 %all-to-all-start = ((s32[16,1,1]{2,1,0:T(1,128)}), s32[16,1,1]{2,1,0:T(1,128)S(1)}, u32[]{:S(2)}, u32[]{:S(2)}) async-start(s32[16,1,1]{2,1,0:T(1,128)} %copy.55), calls=%async_computation | async-start | bytes 16384 | tf_op jit(solution)/shard_map/all_to_all | solution.py:30
  27.2 13.5 %all-to-all-start.1 = ((bf16[16,32,256]{2,1,0:T(8,128)(2,1)}), bf16[16,32,256]{2,1,0:T(8,128)(2,1)S(1)}, u32[]{:S(2)}, u32[]{:S(2)}) async-start(bf16[16,32,256]{2,1,0:T(8,128)(2,1)} %get-tuple-element.31), calls=%async_computation.1 | async-start | bytes 524288 | tf_op jit(solution)/shard_map/all_to_all | solution.py:42
  33.1 9.1 %copy-start.2 = (bf16[16,8,16,128]{3,2,1,0:T(8,128)(2,1)}, bf16[16,8,16,128]{3,2,1,0:T(8,128)(2,1)S(1)}, u32[]{:S(2)}) copy-start(bf16[16,8,16,128]{3,2,1,0:T(8,128)(2,1)S(1)} %copy.80) | copy-start | bytes 1572868
  42.2 2.0 %copy-start = (f32[2,2,512,64,8]{2,3,4,1,0:T(8,128)}, f32[2,2,512,64,8]{2,3,4,1,0:T(8,128)S(1)}, u32[]{:S(2)}) copy-start(f32[2,2,512,64,8]{2,3,4,1,0:T(8,128)S(1)} %fusion.20) | copy-start | bytes 12582916
  49.3 17.8 %all-to-all-start.4 = ((f32[16,32,256]{2,1,0:T(8,128)}), f32[16,32,256]{2,1,0:T(8,128)S(1)}, u32[]{:S(2)}, u32[]{:S(2)}) async-start(f32[16,32,256]{2,1,0:T(8,128)} %bitcast.30), calls=%async_computation.4 | async-start | bytes 1048576 | tf_op jit(solution)/shard_map/all_to_all | solution.py:98
  52.8 25.0 %all-gather.2.cloned.1.call-start = ((), (), s32[]{:S(2)}) async-start(), calls=%async_computation.6 | async-start | bytes 1572864 | tf_op jit(solution)/shard_map/all_gather | solution.py:116
  53.6 108.9 %reduce-scatter.2.cloned.1.call-start = ((), (), s32[]{:S(2)}) async-start(), calls=%async_computation.7 | async-start | bytes 4456448 | tf_op jit(solution)/shard_map/reduce_scatter | solution.py:117
  67.9 9.9 %copy-start.7 = (f32[128,256]{1,0:T(8,128)}, f32[128,256]{1,0:T(8,128)S(1)}, u32[]{:S(2)}) copy-start(f32[128,256]{1,0:T(8,128)S(1)} %reshape.138) | copy-start | bytes 393220
  67.9 29.4 %copy-start.5 = (bf16[128,256]{1,0:T(8,128)(2,1)S(1)}, bf16[128,256]{1,0:T(8,128)(2,1)}, u32[]{:S(2)}) copy-start(bf16[128,256]{1,0:T(8,128)(2,1)} %param.9) | copy-start | bytes 196612
  81.7 16.3 %copy-start.3 = (bf16[16,8,16,128]{3,2,1,0:T(8,128)(2,1)S(1)}, bf16[16,8,16,128]{3,2,1,0:T(8,128)(2,1)}, u32[]{:S(2)}) copy-start(bf16[16,8,16,128]{3,2,1,0:T(8,128)(2,1)} %copy-done.2) | copy-start | bytes 1572868
  98.1 3.9 %copy-start.1 = (f32[2,2,512,64,8]{2,3,4,1,0:T(8,128)S(1)}, f32[2,2,512,64,8]{2,3,4,1,0:T(8,128)}, u32[]{:S(2)}) copy-start(f32[2,2,512,64,8]{2,3,4,1,0:T(8,128)} %copy-done) | copy-start | bytes 12582916
  112.0 23.7 %all-to-all-start.3 = ((f32[16,32,256]{2,1,0:T(8,128)}), f32[16,32,256]{2,1,0:T(8,128)}, u32[]{:S(2)}, u32[]{:S(2)}) async-start(f32[16,32,256]{2,1,0:T(8,128)} %bitcast.81), calls=%async_computation.3 | async-start | bytes 1048576 | tf_op jit(solution)/shard_map/all_to_all | solution.py:97
Sparse Core Ops, SparseCore 0:
  55.2 22.5 all-gather.1
  81.9 80.5 reduce-scatter.1
where the time goes:
time: 172 us; the launch traced here: 171 us
  waiting for transfers between devices  78.9 us (46%)
  local copies, waits for them, and re-layouts  24.1 us (14%)
  starting transfers between devices  18.8 us (11%)
  blocking collectives  15.6 us (9%)
  matrix products  14.8 us (9%)
  between operations  14.4 us (8%)
  other arithmetic  4.43 us (3%)
    reduce_scatter x1, waiting for transfers between devices, local(): lax.psum_scatter(jnp.einsum('td,tc->dc', full_input, value_low, preferred...  24.2 us
    all_to_all x1, waiting for transfers between devices, local(): lax.all_to_all(back_keys, 'kv', split_axis=0, concat_axis=0, tiled=True)  17 us
    all_to_all x1, blocking collectives, local(): lax.all_to_all(send_values, 'kv', split_axis=0, concat_axis=0, tiled=True)  15.6 us
    all_to_all x1, waiting for transfers between devices, local(): lax.all_to_all(back_values, 'kv', split_axis=0, concat_axis=0, tiled=True)  13.5 us
    all_gather x1, waiting for transfers between devices, local(): full_input = lax.all_gather(normed_input, 'tp', axis=1, tiled=True)  9.91 us
    unnamed x23, local copies, waits for them, and re-layouts  8.89 us
    all_to_all x1, waiting for transfers between devices, local(): lax.all_to_all(send_keys, 'kv', split_axis=0, concat_axis=0, tiled=True)  7.44 us
    all_to_all x1, starting transfers between devices, local(): lax.all_to_all(wanted.reshape(devices, 1), 'kv', split_axis=0, concat_axi...  7.39 us
  transfers between devices with their start and end apart: 6, of which 6 were waited for; matrix products, arithmetic and copies ran while one was open for 13% of the time, Pallas kernels for 0%

commit v1 on v0

v1 whole, which is shorter than its diff:
```python
import functools

import jax
import jax.numpy as jnp
from jax import lax
from jax.experimental import pallas as pl
from jax.experimental.pallas import tpu as pltpu
from jax.sharding import PartitionSpec as P

HD = 128
QB = 64
KB = 32
NSEL = 16

MESH = pl.DeviceIdType.MESH
F32 = jnp.float32
BF16 = jnp.bfloat16


def remote(src, dst, send_sem, recv_sem, device_id):
    return pltpu.make_async_remote_copy(
        src_ref=src,
        dst_ref=dst,
        send_sem=send_sem,
        recv_sem=recv_sem,
        device_id=device_id,
        device_id_type=MESH,
    )


class Gather:
    def __init__(self, pool, send_z, send_x, send_c, recv, me, n, xs, upward):
        self.pool, self.recv = pool, recv
        self.send_z, self.send_x, self.send_c = send_z, send_x, send_c
        self.me, self.n, self.xs = me, n, xs
        self.row = 2 * xs
        self.zs = n // self.row
        self.z = me // self.row
        self.r = me % self.row
        self.x = self.r // 2
        self.c = self.r % 2
        self.sends = self.zs - 1 - self.z if upward else self.zs - 1
        self.planes = self.z + 1 if upward else self.zs

    def copy(self, slot, send_sem, dest):
        return remote(
            self.pool.at[slot], self.pool.at[slot], send_sem, self.recv.at[slot], {"kv": dest}
        )

    def plane(self, k):
        return (self.z - k + self.zs) % self.zs

    def along_z(self, k):
        dest = ((self.z + k) % self.zs) * self.row + self.r
        return self.copy(self.me, self.send_z.at[k], dest)

    def along_x(self, k, d):
        slot = self.plane(k) * self.row + self.r
        dest = self.z * self.row + ((self.x + d) % self.xs) * 2 + self.c
        return self.copy(slot, self.send_x.at[k, d], dest)

    def across(self, k, d):
        slot = self.plane(k) * self.row + ((self.x + d) % self.xs) * 2 + self.c
        dest = self.z * self.row + self.x * 2 + (1 - self.c)
        return self.copy(slot, self.send_c.at[k, d], dest)

    def wait_slot(self, slot):
        self.copy(slot, self.send_z.at[0], (self.me + 1) % self.n).wait_recv()

    def start(self):
        def body(k, _):
            self.along_z(k).start()
            return 0

        lax.fori_loop(1, self.sends + 1, body, 0)

    def relay(self):
        def step(k, first):
            slot = self.plane(k) * self.row + self.r
            if not first:
                self.wait_slot(slot)
            for d in range(1, self.xs):
                self.along_x(k, d).start()
            self.across(k, 0).start()

        def cross(k):
            for d in range(1, self.xs):
                slot = self.plane(k) * self.row + ((self.x + d) % self.xs) * 2 + self.c
                self.wait_slot(slot)
                self.across(k, d).start()

        step(0, True)

        def body(k, _):
            step(k, False)
            cross(k - 1)
            return 0

        lax.fori_loop(1, self.planes, body, 0)
        cross(self.planes - 1)

    def finish(self):
        def body(k, _):
            for d in range(self.xs):
                self.wait_slot(
                    self.plane(k) * self.row + ((self.x + d) % self.xs) * 2 + (1 - self.c)
                )
            return 0

        lax.fori_loop(0, self.planes, body, 0)

    def drain(self):
        def zbody(k, _):
            self.along_z(k).wait_send()
            return 0

        lax.fori_loop(1, self.sends + 1, zbody, 0)

        def body(k, _):
            for d in range(1, self.xs):
                self.along_x(k, d).wait_send()
            for d in range(self.xs):
                self.across(k, d).wait_send()
            return 0

        lax.fori_loop(0, self.planes, body, 0)


def dot(a, b, dims):
    return lax.dot_general(a, b, (dims, ((), ())), preferred_element_type=F32)


def kernel(
    n,
    tp,
    chosen_s,
    chosen_v,
    queries,
    keys,
    values,
    lse,
    out_grad,
    normed_t,
    query_grad,
    key_grad,
    value_grad,
    weight_grad,
    pool,
    low_pool,
    norm_pool,
    chosen_all,
    hit,
    sel,
    s_buf,
    d_buf,
    p_low,
    ds_low,
    part,
    back,
    got,
    table,
    local_sem,
    kv_z,
    kv_x,
    kv_c,
    kv_recv,
    lo_z,
    lo_x,
    lo_c,
    lo_recv,
    n_send,
    n_recv,
    c_send,
    c_recv,
    g_send,
    g_recv,
):
    me = lax.axis_index("kv")
    col = lax.axis_index("tp")
    kblocks = keys.shape[0]
    tok = kblocks * KB
    qblocks = tok // QB
    kv_cols = keys.shape[2]
    kv_heads = kv_cols // HD
    group = queries.shape[1] // kv_cols
    rows = normed_t.shape[0] * tp // n
    per = n // tp
    scale = HD ** (-0.5)
    entries = qblocks * NSEL

    own = [
        pltpu.make_async_copy(keys, pool.at[me, 0], local_sem.at[0]),
        pltpu.make_async_copy(values, pool.at[me, 1], local_sem.at[1]),
    ]
    for c in own:
        c.start()

    barrier = pltpu.get_barrier_semaphore()

    def greet(i, _):
        for t in range(tp):
            pl.semaphore_signal(
                barrier, inc=1, device_id={"kv": i, "tp": t}, device_id_type=MESH
            )
        return 0

    lax.fori_loop(0, n, greet, 0)
    for c in own:
        c.wait()
    pl.semaphore_wait(barrier, n * tp)

    kv = Gather(pool, kv_z, kv_x, kv_c, kv_recv, me, n, tp, True)
    kv.start()

    def chosen_copy(i):
        return remote(
            chosen_v, chosen_all.at[me], c_send.at[i], c_recv.at[me], {"kv": i}
        )

    def ask(i, _):
        chosen_copy(i).start()
        return 0

    lax.fori_loop(0, me, ask, 0)
    kv.relay()

    def norm_copy(k, t):
        dest = col * per + k
        return remote(
            normed_t.at[pl.ds(pl.multiple_of(k * rows, rows), rows)],
            norm_pool.at[me],
            n_send.at[k, t],
            n_recv.at[me],
            {"kv": dest, "tp": t},
        )

    def norm_local(k):
        return pltpu.make_async_copy(
            normed_t.at[pl.ds(pl.multiple_of(k * rows, rows), rows)],
            norm_pool.at[me],
            n_recv.at[me],
        )

    def norm_each(act, act_local):
        def body(k0, _):
            k = (k0 + me) % per
            for t in range(tp):
                self_dest = (col * per + k == me) & (col == t)

                @pl.when(self_dest)
                def _():
                    act_local(k)

                @pl.when(jnp.logical_not(self_dest))
                def _():
                    act(k, t)

            return 0

        lax.fori_loop(0, per, body, 0)

    norm_each(lambda k, t: norm_copy(k, t).start(), lambda k: norm_local(k).start())

    def look(i, _):
        for b in range(qblocks):
            found = jnp.int32(entries)
            for e in range(NSEL):
                found = jnp.where(chosen_s[b, e] // kblocks == i, b * NSEL + e, found)
            table[b, i] = found
        return 0

    lax.fori_loop(0, me, look, 0)
    for w in range(kblocks):
        for b in range(qblocks):
            found = jnp.int32(entries)
            for e in range(NSEL):
                found = jnp.where(chosen_s[b, e] == me * kblocks + w, b * NSEL + e, found)
            table[b, n + w] = found
    part[:, entries] = jnp.zeros_like(part[:, entries])

    kv.finish()
    plane_end = (kv.z + 1) * kv.row * kblocks
    span = NSEL * KB
    width = group * QB
    key_iota = lax.broadcasted_iota(jnp.int32, (KB, width), 0)
    row_iota = lax.broadcasted_iota(jnp.int32, (KB, width), 1) % QB
    for b in range(qblocks):
        for e in range(NSEL):
            block = chosen_s[b, e]
            block = jnp.where(block < plane_end, block, 0)
            for a in range(2):
                sel[a, e * KB : (e + 1) * KB, :] = pool[block // kblocks, a, block % kblocks]
        for g in range(kv_heads):
            lanes = slice(g * HD, (g + 1) * HD)

            def stack(ref):
                return jnp.concatenate(
                    [
                        ref[b * QB : (b + 1) * QB, (g * group + h) * HD : (g * group + h + 1) * HD]
                        for h in range(group)
                    ],
                    axis=0,
                )

            q = stack(queries)
            do = stack(out_grad)
            k_sel = sel[0, :, lanes]
            s_buf[...] = dot(k_sel, q, ((1,), (1,)))
            d_buf[...] = dot(sel[1, :, lanes], do, ((1,), (1,)))
            log = lse[b, g]
            delta = jnp.zeros((8, width), F32)
            for e in range(NSEL):
                at = slice(e * KB, (e + 1) * KB)
                limit = (me * tok + b * QB) - chosen_s[b, e] * KB
                valid = key_iota - row_iota <= limit
                p = jnp.where(valid, jnp.exp(s_buf[at, :] * scale - log), 0.0)
                s_buf[at, :] = p
                p_low[at, :] = p.astype(BF16)
                pd = p * d_buf[at, :]
                delta = delta + jnp.sum(pd.reshape(KB // 8, 8, width), axis=0)
            delta = jnp.sum(delta, axis=0, keepdims=True)
            for e in range(NSEL):
                at = slice(e * KB, (e + 1) * KB)
                ds_low[at, :] = (s_buf[at, :] * (d_buf[at, :] - delta)).astype(BF16)
            ds = ds_low[...]
            here = slice(b * NSEL, (b + 1) * NSEL)
            part[0, here, :, lanes] = (dot(ds, q, ((1,), (0,))) * scale).reshape(NSEL, KB, HD)
            part[1, here, :, lanes] = dot(p_low[...], do, ((1,), (0,))).reshape(NSEL, KB, HD)
            dq = dot(ds, k_sel, ((0,), (0,))) * scale
            for h in range(group):
                query_grad[
                    b * QB : (b + 1) * QB, (g * group + h) * HD : (g * group + h + 1) * HD
                ] = dq[h * QB : (h + 1) * QB]

    def back_copy(i):
        return remote(back.at[i], got.at[me], g_send.at[i], g_recv.at[me], {"kv": i})

    def send_back(i, _):
        for a in range(2):
            total = part[a, table[0, i]]
            for b in range(1, qblocks):
                total = total + part[a, table[b, i]]
            back[i, a] = total.astype(BF16)
        back_copy(i).start()
        return 0

    lax.fori_loop(0, me, send_back, 0)

    for w in range(kblocks):
        for a, out in ((0, key_grad), (1, value_grad)):
            total = part[a, table[0, n + w]]
            for b in range(1, qblocks):
                total = total + part[a, table[b, n + w]]
            out[w] = total

    def heard(j, _):
        remote(
            chosen_v, chosen_all.at[j], c_send.at[0], c_recv.at[j], {"kv": (me + 1) % n}
        ).wait_recv()
        for w in range(kblocks):
            named = jnp.where(chosen_all[j] == me * kblocks + w, 1.0, 0.0)
            named = jnp.max(jnp.max(named, axis=1, keepdims=True), axis=0, keepdims=True)
            hit[j, w] = jnp.broadcast_to(named, (8, kv_cols))
        return 0

    lax.fori_loop(me + 1, n, heard, 0)

    def add_back(j, _):
        remote(
            back.at[0], got.at[j], g_send.at[0], g_recv.at[j], {"kv": (me + 1) % n}
        ).wait_recv()
        terms = [got[j, a].astype(F32) for a in range(2)]
        for w in range(kblocks):
            mask = jnp.concatenate([hit[j, w]] * (KB // 8), axis=0)
            for a, out in ((0, key_grad), (1, value_grad)):
                out[w] += mask * terms[a]
        return 0

    lax.fori_loop(me + 1, n, add_back, 0)

    low_pool[me] = value_grad[...].reshape(tok, kv_cols).astype(BF16)
    low = Gather(low_pool, lo_z, lo_x, lo_c, lo_recv, me, n, tp, False)
    low.start()
    low.relay()

    def norm_wait(j, _):
        pltpu.make_async_copy(norm_pool.at[j], norm_pool.at[j], n_recv.at[j]).wait()
        return 0

    lax.fori_loop(0, n, norm_wait, 0)
    low.finish()

    row = kv.row

    def product(z):
        a = jnp.concatenate([norm_pool[z * row + i] for i in range(row)], axis=1)
        v = jnp.concatenate([low_pool[z * row + i] for i in range(row)], axis=0)
        return dot(a, v, ((1,), (0,)))

    weight_grad[...] = product(0)

    def weigh(z, _):
        weight_grad[...] += product(z)
        return 0

    lax.fori_loop(1, kv.zs, weigh, 0)

    kv.drain()
    low.drain()

    def drain_small(i, _):
        chosen_copy(i).wait_send()
        back_copy(i).wait_send()
        return 0

    lax.fori_loop(0, me, drain_small, 0)
    norm_each(lambda k, t: norm_copy(k, t).wait_send(), lambda k: None)


def local(n, tp, queries, keys, values, logsum, out_grad, normed_input, chosen):
    tok, kv_cols = keys.shape
    kv_heads = kv_cols // HD
    group = queries.shape[1] // kv_cols
    kblocks = tok // KB
    qblocks = tok // QB
    rows = normed_input.shape[1] * tp // n
    zs = n // (2 * tp)
    entries = qblocks * NSEL
    span = NSEL * KB
    width = group * QB
    lse = (
        logsum.reshape(qblocks, QB, kv_heads, group)
        .transpose(0, 2, 3, 1)
        .reshape(qblocks, kv_heads, 1, width)
    )
    vmem = pl.BlockSpec(memory_space=pltpu.VMEM)
    dma = pltpu.SemaphoreType.DMA
    outs = pl.pallas_call(
        functools.partial(kernel, n, tp),
        out_shape=(
            jax.ShapeDtypeStruct((tok, queries.shape[1]), F32),
            jax.ShapeDtypeStruct((kblocks, KB, kv_cols), F32),
            jax.ShapeDtypeStruct((kblocks, KB, kv_cols), F32),
            jax.ShapeDtypeStruct((rows, kv_cols), F32),
        ),
        in_specs=[pl.BlockSpec(memory_space=pltpu.SMEM)] + [vmem] * 7,
        out_specs=(vmem,) * 4,
        scratch_shapes=[
            pltpu.VMEM((n, 2, kblocks, KB, kv_cols), BF16),
            pltpu.VMEM((n, tok, kv_cols), BF16),
            pltpu.VMEM((n, rows, tok), BF16),
            pltpu.VMEM((n, qblocks, NSEL), jnp.int32),
            pltpu.VMEM((n, kblocks, 8, kv_cols), F32),
            pltpu.VMEM((2, span, kv_cols), BF16),
            pltpu.VMEM((span, width), F32),
            pltpu.VMEM((span, width), F32),
            pltpu.VMEM((span, width), BF16),
            pltpu.VMEM((span, width), BF16),
            pltpu.VMEM((2, entries + 1, KB, kv_cols), F32),
            pltpu.VMEM((n, 2, KB, kv_cols), BF16),
            pltpu.VMEM((n, 2, KB, kv_cols), BF16),
            pltpu.SMEM((qblocks, n + kblocks), jnp.int32),
            dma((2,)),
            dma((zs,)),
            dma((zs, tp)),
            dma((zs, tp)),
            dma((n,)),
            dma((zs,)),
            dma((zs, tp)),
            dma((zs, tp)),
            dma((n,)),
            dma((n // tp, tp)),
            dma((n,)),
            dma((n,)),
            dma((n,)),
            dma((n,)),
            dma((n,)),
        ],
        compiler_params=pltpu.CompilerParams(
            collective_id=0, has_side_effects=True, vmem_limit_bytes=60 * 1024 * 1024
        ),
        name="attention_back",
    )(
        chosen,
        chosen,
        queries,
        keys.reshape(kblocks, KB, kv_cols),
        values.reshape(kblocks, KB, kv_cols),
        lse,
        out_grad,
        normed_input.T,
    )
    query_grad, key_grad, value_grad, weight_grad = outs
    return (
        query_grad,
        key_grad.reshape(tok, kv_cols),
        value_grad.reshape(tok, kv_cols),
        weight_grad,
    )


def solution(mesh):
    n, tp = mesh.shape["kv"], mesh.shape["tp"]
    in_specs = (P("kv", "tp"),) * 6 + (P("kv", None),)
    out_specs = (P("kv", "tp"),) * 4
    return jax.shard_map(
        functools.partial(local, n, tp),
        mesh=mesh,
        in_specs=in_specs,
        out_specs=out_specs,
        check_vma=False,
    )
```

time: 172 us -> 106 us (0.62)
  the two profiles are of different devices: /device:TPU:0 before, /device:TPU:17 now
where the time goes in v1:
time: 106 us
  Pallas kernels  97.4 us (92%)
  local copies, waits for them, and re-layouts  7.86 us (7%)
    pallas_call x1, Pallas kernels, local(): pl.pallas_call(functools.partial(kernel, n, tp), out_shape=(jax.ShapeDtyp...  97.4 us
    unnamed x11, local copies, waits for them, and re-layouts  6.4 us

profile of v1, /device:TPU:17, one launch (start us, length us, event | category | flops | bytes accessed | tf_op | source)
XLA Modules:
  0.0 105.9 jit_solution(1550748522781026538)
XLA Ops:
  0.6 0.8 reshape.28
  1.4 0.7 reshape.29.lse
  2.1 2.0 %copy.12 = bf16[128,2048]{0,1:T(8,128)(2,1)} copy(bf16[128,2048]{1,0:T(8,128)(2,1)} %param.12) | data formatting | bytes 1048576 | tf_op args[5]
  4.1 97.4 %attention_back.1 = (f32[128,2048]{1,0:T(8,128)}, f32[4,32,256]{2,1,0:T(8,128)}, f32[4,32,256]{2,1,0:T(8,128)}, f32[256,256]{1,0:T(8,128)}) custom-call(s32[2,16]{1,0:T(2,128)} %chosen_v.1, s32[2,16]{1,0:T(2,128)} %chosen_v.1, bf16[128,2048]{1,0:T(8,128)(2,1)} %queries.1, bf16[4,32,256]{2,1,0:T(8,128)(2,1)} %bitcast.16, bf16[4,32,256]{2,1,0:T(8,128)(2,1)} %bitcast.17, ...), custom_call_target="tpu_custom_call" | custom-call | tf_op jit(solution)/shard_map/attention_back/pallas_call | solution.py:438
  101.5 0.0 copy-start.2
  101.5 0.0 copy-start.1
  101.6 2.3 %copy.19 = f32[128,2048]{1,0:T(8,128)} copy(f32[128,2048]{1,0:T(8,128)} %get-tuple-element.16) | data formatting | bytes 2097152
  103.9 0.0 copy-done.2
  103.9 0.0 copy-start
  103.9 0.7 copy.20
  104.6 0.0 copy-done.1
  104.6 0.7 copy.21
  105.2 0.0 copy-done
  105.2 0.7 copy.22
  (1 shorter events, 0.0 us)
Async XLA Ops:
  101.5 2.4 %copy-start.2 = (f32[4,32,256]{2,1,0:T(8,128)S(1)}, f32[4,32,256]{2,1,0:T(8,128)}, u32[]{:S(2)}) copy-start(f32[4,32,256]{2,1,0:T(8,128)} %get-tuple-element.9) | copy-start | bytes 393220
  101.5 3.0 %copy-start.1 = (f32[4,32,256]{2,1,0:T(8,128)S(1)}, f32[4,32,256]{2,1,0:T(8,128)}, u32[]{:S(2)}) copy-start(f32[4,32,256]{2,1,0:T(8,128)} %get-tuple-element.10) | copy-start | bytes 393220
  103.9 1.3 %copy-start = (f32[256,256]{1,0:T(8,128)S(1)}, f32[256,256]{1,0:T(8,128)}, u32[]{:S(2)}) copy-start(f32[256,256]{1,0:T(8,128)} %get-tuple-element.19) | copy-start | bytes 786436

commit v2 on v1

--- a/solution.py
+++ b/solution.py
@@ -29,7 +29,7 @@
 
 
 class Gather:
-    def __init__(self, pool, send_z, send_x, send_c, recv, me, n, xs, upward):
+    def __init__(self, pool, send_z, send_x, send_c, recv, me, n, xs):
         self.pool, self.recv = pool, recv
         self.send_z, self.send_x, self.send_c = send_z, send_x, send_c
         self.me, self.n, self.xs = me, n, xs
@@ -39,8 +39,8 @@
         self.r = me % self.row
         self.x = self.r // 2
         self.c = self.r % 2
-        self.sends = self.zs - 1 - self.z if upward else self.zs - 1
-        self.planes = self.z + 1 if upward else self.zs
+        self.sends = self.zs - 1
+        self.planes = self.zs
 
     def copy(self, slot, send_sem, dest):
         return remote(
@@ -133,23 +133,25 @@
 def kernel(
     n,
     tp,
-    chosen_s,
-    chosen_v,
+    chosen,
     queries,
     keys,
     values,
-    lse,
+    logsum,
     out_grad,
-    normed_t,
+    normed,
     query_grad,
     key_grad,
     value_grad,
     weight_grad,
     pool,
+    ask,
+    asked,
+    give,
     low_pool,
+    norm_parts,
+    norm_via,
     norm_pool,
-    chosen_all,
-    hit,
     sel,
     s_buf,
     d_buf,
@@ -160,20 +162,22 @@
     got,
     table,
     local_sem,
-    kv_z,
-    kv_x,
-    kv_c,
+    ask_send,
+    ask_recv,
+    kv_send,
     kv_recv,
+    back_send,
+    back_recv,
+    via_send,
+    via_recv,
+    norm_send,
+    norm_recv,
+    swap_send,
+    swap_recv,
     lo_z,
     lo_x,
     lo_c,
     lo_recv,
-    n_send,
-    n_recv,
-    c_send,
-    c_recv,
-    g_send,
-    g_recv,
 ):
     me = lax.axis_index("kv")
     col = lax.axis_index("tp")
@@ -183,17 +187,12 @@
     kv_cols = keys.shape[2]
     kv_heads = kv_cols // HD
     group = queries.shape[1] // kv_cols
-    rows = normed_t.shape[0] * tp // n
     per = n // tp
+    sub = norm_parts.shape[2]
+    rows = sub * tp
     scale = HD ** (-0.5)
     entries = qblocks * NSEL
-
-    own = [
-        pltpu.make_async_copy(keys, pool.at[me, 0], local_sem.at[0]),
-        pltpu.make_async_copy(values, pool.at[me, 1], local_sem.at[1]),
-    ]
-    for c in own:
-        c.start()
+    after = (me + 1) % n
 
     barrier = pltpu.get_barrier_semaphore()
 
@@ -205,91 +204,133 @@
         return 0
 
     lax.fori_loop(0, n, greet, 0)
-    for c in own:
-        c.wait()
-    pl.semaphore_wait(barrier, n * tp)
-
-    kv = Gather(pool, kv_z, kv_x, kv_c, kv_recv, me, n, tp, True)
-    kv.start()
-
-    def chosen_copy(i):
-        return remote(
-            chosen_v, chosen_all.at[me], c_send.at[i], c_recv.at[me], {"kv": i}
-        )
-
-    def ask(i, _):
-        chosen_copy(i).start()
-        return 0
-
-    lax.fori_loop(0, me, ask, 0)
-    kv.relay()
-
-    def norm_copy(k, t):
-        dest = col * per + k
-        return remote(
-            normed_t.at[pl.ds(pl.multiple_of(k * rows, rows), rows)],
-            norm_pool.at[me],
-            n_send.at[k, t],
-            n_recv.at[me],
-            {"kv": dest, "tp": t},
-        )
-
-    def norm_local(k):
-        return pltpu.make_async_copy(
-            normed_t.at[pl.ds(pl.multiple_of(k * rows, rows), rows)],
-            norm_pool.at[me],
-            n_recv.at[me],
-        )
-
-    def norm_each(act, act_local):
-        def body(k0, _):
-            k = (k0 + me) % per
-            for t in range(tp):
-                self_dest = (col * per + k == me) & (col == t)
-
-                @pl.when(self_dest)
-                def _():
-                    act_local(k)
-
-                @pl.when(jnp.logical_not(self_dest))
-                def _():
-                    act(k, t)
-
-            return 0
-
-        lax.fori_loop(0, per, body, 0)
-
-    norm_each(lambda k, t: norm_copy(k, t).start(), lambda k: norm_local(k).start())
+    own = []
+    for w in range(kblocks):
+        for a, ref in ((0, keys), (1, values)):
+            c = pltpu.make_async_copy(ref.at[w], pool.at[n + w, a], local_sem.at[w, a])
+            c.start()
+            own.append(c)
 
     def look(i, _):
+        block = jnp.int32(0)
         for b in range(qblocks):
             found = jnp.int32(entries)
             for e in range(NSEL):
-                found = jnp.where(chosen_s[b, e] // kblocks == i, b * NSEL + e, found)
+                c = chosen[b, e]
+                here = c // kblocks == i
+                found = jnp.where(here, b * NSEL + e, found)
+                block = jnp.where(here, c % kblocks + 1, block)
             table[b, i] = found
+        ask[i] = jnp.full(ask.shape[1:], block, jnp.int32)
         return 0
 
     lax.fori_loop(0, me, look, 0)
+    for m in range(normed.shape[1] // HD):
+        turned = normed[:, m * HD : (m + 1) * HD].T
+        for p in range(0, HD, sub):
+            at = m * HD + p
+            norm_parts[at % rows // sub, at // rows] = turned[p : p + sub]
+
+    pl.semaphore_wait(barrier, n * tp)
+
+    def ask_copy(i):
+        return remote(ask.at[i], asked.at[me], ask_send.at[i], ask_recv.at[me], {"kv": i})
+
+    def ask_start(i, _):
+        ask_copy(i).start()
+        return 0
+
+    lax.fori_loop(0, me, ask_start, 0)
+
+    def via_copy(d):
+        q = (col + d) % tp
+        return remote(
+            norm_parts.at[q], norm_via.at[d], via_send.at[d], via_recv.at[d], {"tp": q}
+        )
+
+    for d in range(1, tp):
+        via_copy(d).start()
+
     for w in range(kblocks):
         for b in range(qblocks):
             found = jnp.int32(entries)
             for e in range(NSEL):
-                found = jnp.where(chosen_s[b, e] == me * kblocks + w, b * NSEL + e, found)
+                found = jnp.where(chosen[b, e] == me * kblocks + w, b * NSEL + e, found)
             table[b, n + w] = found
     part[:, entries] = jnp.zeros_like(part[:, entries])
 
-    kv.finish()
-    plane_end = (kv.z + 1) * kv.row * kblocks
+    def kv_copy(j):
+        return remote(give.at[j], pool.at[me], kv_send.at[j], kv_recv.at[me], {"kv": j})
+
+    def answer(k, _):
+        j = n - 1 - k
+        remote(ask.at[0], asked.at[j], ask_send.at[0], ask_recv.at[j], {"kv": after}).wait_recv()
+        named = asked[j]
+        for a, ref in ((0, keys), (1, values)):
+            block = jnp.zeros((KB, kv_cols), F32)
+            for w in range(kblocks):
+                mask = jnp.concatenate([named == w + 1] * (KB // 8), axis=0)
+                block = jnp.where(mask, ref[w].astype(F32), block)
+            give[j, a] = block.astype(BF16)
+        kv_copy(j).start()
+        return 0
+
+    lax.fori_loop(0, n - 1 - me, answer, 0)
+
+    def norm_each(act, act_local):
+        def body(k0, _):
+            for d in range(tp):
+                t = (col + tp - d) % tp
+                k = (k0 + me) % per
+                dest = t * per + k
+                src = norm_parts.at[col, k] if d == 0 else norm_via.at[d, k]
+
+                @pl.when(dest == me)
+                def _():
+                    act_local(
+                        pltpu.make_async_copy(src, norm_pool.at[col, me], norm_recv.at[me])
+                    )
+
+                @pl.when(dest != me)
+                def _():
+                    act(
+                        remote(
+                            src,
+                            norm_pool.at[col, me],
+                            norm_send.at[d, k],
+                            norm_recv.at[me],
+                            {"kv": dest},
+                        )
+                    )
+
+            return 0
+
+        lax.fori_loop(0, per, body, 0)
+
+    for d in range(1, tp):
+        via_copy(d).wait_recv()
+    norm_each(lambda c: c.start(), lambda c: c.start())
+
+    for c in own:
+        c.wait()
+
+    def kv_wait(j, _):
+        remote(give.at[0], pool.at[j], kv_send.at[0], kv_recv.at[j], {"kv": after}).wait_recv()
+        return 0
+
+    lax.fori_loop(0, me, kv_wait, 0)
     span = NSEL * KB
     width = group * QB
     key_iota = lax.broadcasted_iota(jnp.int32, (KB, width), 0)
     row_iota = lax.broadcasted_iota(jnp.int32, (KB, width), 1) % QB
+    logs = logsum[...].T
     for b in range(qblocks):
         for e in range(NSEL):
-            block = chosen_s[b, e]
-            block = jnp.where(block < plane_end, block, 0)
+            block = chosen[b, e]
+            owner = block // kblocks
+            slot = jnp.where(owner == me, n + block % kblocks, jnp.where(owner < me, owner, n))
             for a in range(2):
-                sel[a, e * KB : (e + 1) * KB, :] = pool[block // kblocks, a, block % kblocks]
+                sel[a, e * KB : (e + 1) * KB, :] = pool[slot, a]
         for g in range(kv_heads):
             lanes = slice(g * HD, (g + 1) * HD)
 
@@ -307,11 +348,17 @@
             k_sel = sel[0, :, lanes]
             s_buf[...] = dot(k_sel, q, ((1,), (1,)))
             d_buf[...] = dot(sel[1, :, lanes], do, ((1,), (1,)))
-            log = lse[b, g]
+            log = jnp.concatenate(
+                [
+                    logs[g * group + h : g * group + h + 1, b * QB : (b + 1) * QB]
+                    for h in range(group)
+                ],
+                axis=1,
+            )
             delta = jnp.zeros((8, width), F32)
             for e in range(NSEL):
                 at = slice(e * KB, (e + 1) * KB)
-                limit = (me * tok + b * QB) - chosen_s[b, e] * KB
+                limit = (me * tok + b * QB) - chosen[b, e] * KB
                 valid = key_iota - row_iota <= limit
                 p = jnp.where(valid, jnp.exp(s_buf[at, :] * scale - log), 0.0)
                 s_buf[at, :] = p
@@ -333,7 +380,7 @@
                 ] = dq[h * QB : (h + 1) * QB]
 
     def back_copy(i):
-        return remote(back.at[i], got.at[me], g_send.at[i], g_recv.at[me], {"kv": i})
+        return remote(back.at[i], got.at[me], back_send.at[i], back_recv.at[me], {"kv": i})
 
     def send_back(i, _):
         for a in range(2):
@@ -353,68 +400,82 @@
                 total = total + part[a, table[b, n + w]]
             out[w] = total
 
-    def heard(j, _):
-        remote(
-            chosen_v, chosen_all.at[j], c_send.at[0], c_recv.at[j], {"kv": (me + 1) % n}
-        ).wait_recv()
-        for w in range(kblocks):
-            named = jnp.where(chosen_all[j] == me * kblocks + w, 1.0, 0.0)
-            named = jnp.max(jnp.max(named, axis=1, keepdims=True), axis=0, keepdims=True)
-            hit[j, w] = jnp.broadcast_to(named, (8, kv_cols))
-        return 0
-
-    lax.fori_loop(me + 1, n, heard, 0)
+    def swap_copy(d):
+        q = (col + d) % tp
+        return remote(
+            norm_pool.at[col], norm_pool.at[col], swap_send.at[d], swap_recv.at[d], {"tp": q}
+        )
+
+    def norm_wait(j, _):
+        pltpu.make_async_copy(
+            norm_pool.at[col, j], norm_pool.at[col, j], norm_recv.at[j]
+        ).wait()
+        return 0
+
+    lax.fori_loop(0, n, norm_wait, 0)
+    for d in range(1, tp):
+        swap_copy(d).start()
 
     def add_back(j, _):
         remote(
-            back.at[0], got.at[j], g_send.at[0], g_recv.at[j], {"kv": (me + 1) % n}
+            back.at[0], got.at[j], back_send.at[0], back_recv.at[j], {"kv": after}
         ).wait_recv()
+        named = asked[j]
         terms = [got[j, a].astype(F32) for a in range(2)]
         for w in range(kblocks):
-            mask = jnp.concatenate([hit[j, w]] * (KB // 8), axis=0)
+            mask = jnp.concatenate([named == w + 1] * (KB // 8), axis=0)
             for a, out in ((0, key_grad), (1, value_grad)):
-                out[w] += mask * terms[a]
+                out[w] += jnp.where(mask, terms[a], 0.0)
         return 0
 
     lax.fori_loop(me + 1, n, add_back, 0)
 
     low_pool[me] = value_grad[...].reshape(tok, kv_cols).astype(BF16)
-    low = Gather(low_pool, lo_z, lo_x, lo_c, lo_recv, me, n, tp, False)
+    low = Gather(low_pool, lo_z, lo_x, lo_c, lo_recv, me, n, tp)
     low.start()
     low.relay()
-
-    def norm_wait(j, _):
-        pltpu.make_async_copy(norm_pool.at[j], norm_pool.at[j], n_recv.at[j]).wait()
-        return 0
-
-    lax.fori_loop(0, n, norm_wait, 0)
+    for d in range(1, tp):
+        q = (col + tp - d) % tp
+        remote(
+            norm_pool.at[q], norm_pool.at[q], swap_send.at[d], swap_recv.at[d], {"tp": q}
+        ).wait_recv()
     low.finish()
 
-    row = kv.row
-
-    def product(z):
-        a = jnp.concatenate([norm_pool[z * row + i] for i in range(row)], axis=1)
+    row = low.row
+
+    def product(z, q):
+        a = jnp.concatenate([norm_pool[q, z * row + i] for i in range(row)], axis=1)
         v = jnp.concatenate([low_pool[z * row + i] for i in range(row)], axis=0)
         return dot(a, v, ((1,), (0,)))
 
-    weight_grad[...] = product(0)
+    for q in range(tp):
+        weight_grad[q * sub : (q + 1) * sub] = product(0, q)
 
     def weigh(z, _):
-        weight_grad[...] += product(z)
-        return 0
-
-    lax.fori_loop(1, kv.zs, weigh, 0)
-
-    kv.drain()
+        for q in range(tp):
+            weight_grad[q * sub : (q + 1) * sub] += product(z, q)
+        return 0
+
+    lax.fori_loop(1, low.zs, weigh, 0)
+
     low.drain()
 
-    def drain_small(i, _):
-        chosen_copy(i).wait_send()
+    def drain_early(i, _):
+        ask_copy(i).wait_send()
         back_copy(i).wait_send()
         return 0
 
-    lax.fori_loop(0, me, drain_small, 0)
-    norm_each(lambda k, t: norm_copy(k, t).wait_send(), lambda k: None)
+    lax.fori_loop(0, me, drain_early, 0)
+
+    def drain_late(j, _):
+        kv_copy(j).wait_send()
+        return 0
+
+    lax.fori_loop(me + 1, n, drain_late, 0)
+    for d in range(1, tp):
+        via_copy(d).wait_send()
+        swap_copy(d).wait_send()
+    norm_each(lambda c: c.wait_send(), lambda c: None)
 
 
 def local(n, tp, queries, keys, values, logsum, out_grad, normed_input, chosen):
@@ -428,11 +489,7 @@
     entries = qblocks * NSEL
     span = NSEL * KB
     width = group * QB
-    lse = (
-        logsum.reshape(qblocks, QB, kv_heads, group)
-        .transpose(0, 2, 3, 1)
-        .reshape(qblocks, kv_heads, 1, width)
-    )
+    per = n // tp
     vmem = pl.BlockSpec(memory_space=pltpu.VMEM)
     dma = pltpu.SemaphoreType.DMA
     outs = pl.pallas_call(
@@ -443,14 +500,17 @@
             jax.ShapeDtypeStruct((kblocks, KB, kv_cols), F32),
             jax.ShapeDtypeStruct((rows, kv_cols), F32),
         ),
-        in_specs=[pl.BlockSpec(memory_space=pltpu.SMEM)] + [vmem] * 7,
+        in_specs=[pl.BlockSpec(memory_space=pltpu.SMEM)] + [vmem] * 6,
         out_specs=(vmem,) * 4,
         scratch_shapes=[
-            pltpu.VMEM((n, 2, kblocks, KB, kv_cols), BF16),
+            pltpu.VMEM((n + kblocks, 2, KB, kv_cols), BF16),
+            pltpu.VMEM((n, 8, kv_cols), jnp.int32),
+            pltpu.VMEM((n, 8, kv_cols), jnp.int32),
+            pltpu.VMEM((n, 2, KB, kv_cols), BF16),
             pltpu.VMEM((n, tok, kv_cols), BF16),
-            pltpu.VMEM((n, rows, tok), BF16),
-            pltpu.VMEM((n, qblocks, NSEL), jnp.int32),
-            pltpu.VMEM((n, kblocks, 8, kv_cols), F32),
+            pltpu.VMEM((tp, per, rows // tp, tok), BF16),
+            pltpu.VMEM((tp, per, rows // tp, tok), BF16),
+            pltpu.VMEM((tp, n, rows // tp, tok), BF16),
             pltpu.VMEM((2, span, kv_cols), BF16),
             pltpu.VMEM((span, width), F32),
             pltpu.VMEM((span, width), F32),
@@ -460,20 +520,22 @@
             pltpu.VMEM((n, 2, KB, kv_cols), BF16),
             pltpu.VMEM((n, 2, KB, kv_cols), BF16),
             pltpu.SMEM((qblocks, n + kblocks), jnp.int32),
-            dma((2,)),
+            dma((kblocks, 2)),
+            dma((n,)),
+            dma((n,)),
+            dma((n,)),
+            dma((n,)),
+            dma((n,)),
+            dma((n,)),
+            dma((tp,)),
+            dma((tp,)),
+            dma((tp, per)),
+            dma((n,)),
+            dma((tp,)),
+            dma((tp,)),
             dma((zs,)),
             dma((zs, tp)),
             dma((zs, tp)),
-            dma((n,)),
-            dma((zs,)),
-            dma((zs, tp)),
-            dma((zs, tp)),
-            dma((n,)),
-            dma((n // tp, tp)),
-            dma((n,)),
-            dma((n,)),
-            dma((n,)),
-            dma((n,)),
             dma((n,)),
         ],
         compiler_params=pltpu.CompilerParams(
@@ -482,13 +544,12 @@
         name="attention_back",
     )(
         chosen,
-        chosen,
         queries,
         keys.reshape(kblocks, KB, kv_cols),
         values.reshape(kblocks, KB, kv_cols),
-        lse,
+        logsum,
         out_grad,
-        normed_input.T,
+        normed_input,
     )
     query_grad, key_grad, value_grad, weight_grad = outs
     return (

time: 106 us -> 65.7 us (0.62)
  the two profiles are of different devices: /device:TPU:17 before, /device:TPU:23 now
where the time goes in v2:
time: 65.7 us; the launch traced here: 65.5 us
  Pallas kernels  59 us (90%)
  local copies, waits for them, and re-layouts  5.79 us (9%)
  between operations  0.66 us (1%)
    pallas_call x1, Pallas kernels, local(): pl.pallas_call(functools.partial(kernel, n, tp), out_shape=(jax.ShapeDtyp...  59 us
    unnamed x11, local copies, waits for them, and re-layouts  5.79 us

profile of v2, /device:TPU:23, one launch (start us, length us, event | category | flops | bytes accessed | tf_op | source)
XLA Modules:
  0.0 65.5 jit_solution(7148925575105676344)
XLA Ops:
  0.6 1.4 %copy.11.logsum = f32[128,16]{1,0:T(8,128)} copy(f32[128,16]{0,1:T(8,128)} %param.10) | data formatting | bytes 16384 | tf_op args[3]
  2.1 59.0 %attention_back.1 = (f32[128,2048]{1,0:T(8,128)}, f32[4,32,256]{2,1,0:T(8,128)}, f32[4,32,256]{2,1,0:T(8,128)}, f32[256,256]{1,0:T(8,128)}) custom-call(s32[2,16]{1,0:T(2,128)} %chosen.1, bf16[128,2048]{1,0:T(8,128)(2,1)} %queries.1, bf16[4,32,256]{2,1,0:T(8,128)(2,1)} %bitcast.6, bf16[4,32,256]{2,1,0:T(8,128)(2,1)} %bitcast.7, f32[128,16]{1,0:T(8,128)} %copy.11.logsum, ...), custom_call_target="tpu_custom_call" | custom-call | tf_op jit(solution)/shard_map/attention_back/pallas_call | solution.py:495
  61.1 0.0 copy-start.2
  61.1 0.0 copy-start.1
  61.1 2.3 %copy.16 = f32[128,2048]{1,0:T(8,128)} copy(f32[128,2048]{1,0:T(8,128)} %get-tuple-element.16) | data formatting | bytes 2097152
  63.5 0.0 copy-done.2
  63.5 0.0 copy-start
  63.5 0.7 %copy.17 = f32[128,256]{1,0:T(8,128)} copy(f32[128,256]{1,0:T(8,128)S(1)} %bitcast.5) | data formatting | bytes 262144
  64.1 0.0 copy-done.1
  64.1 0.7 %copy.18 = f32[128,256]{1,0:T(8,128)} copy(f32[128,256]{1,0:T(8,128)S(1)} %bitcast.4) | data formatting | bytes 262144
  64.8 0.0 copy-done
  64.8 0.7 %copy.19 = f32[256,256]{1,0:T(8,128)} copy(f32[256,256]{1,0:T(8,128)S(1)} %copy-done) | data formatting | bytes 524288
Async XLA Ops:
  61.1 2.4 %copy-start.2 = (f32[4,32,256]{2,1,0:T(8,128)S(1)}, f32[4,32,256]{2,1,0:T(8,128)}, u32[]{:S(2)}) copy-start(f32[4,32,256]{2,1,0:T(8,128)} %get-tuple-element.9) | copy-start | bytes 393220
  61.1 3.0 %copy-start.1 = (f32[4,32,256]{2,1,0:T(8,128)S(1)}, f32[4,32,256]{2,1,0:T(8,128)}, u32[]{:S(2)}) copy-start(f32[4,32,256]{2,1,0:T(8,128)} %get-tuple-element.10) | copy-start | bytes 393220
  63.5 1.3 %copy-start = (f32[256,256]{1,0:T(8,128)S(1)}, f32[256,256]{1,0:T(8,128)}, u32[]{:S(2)}) copy-start(f32[256,256]{1,0:T(8,128)} %get-tuple-element.19) | copy-start | bytes 786436

commit v3 on v2

--- a/solution.py
+++ b/solution.py
@@ -144,7 +144,6 @@
     key_grad,
     value_grad,
     weight_grad,
-    pool,
     ask,
     asked,
     give,
@@ -178,6 +177,7 @@
     lo_x,
     lo_c,
     lo_recv,
+    *pools,
 ):
     me = lax.axis_index("kv")
     col = lax.axis_index("tp")
@@ -207,9 +207,14 @@
     own = []
     for w in range(kblocks):
         for a, ref in ((0, keys), (1, values)):
-            c = pltpu.make_async_copy(ref.at[w], pool.at[n + w, a], local_sem.at[w, a])
-            c.start()
-            own.append(c)
+            for g in range(kv_heads):
+                c = pltpu.make_async_copy(
+                    ref.at[w, :, g * HD : (g + 1) * HD],
+                    pools[g].at[n + w, a],
+                    local_sem.at[g, w, a],
+                )
+                c.start()
+                own.append(c)
 
     def look(i, _):
         block = jnp.int32(0)
@@ -257,41 +262,49 @@
             for e in range(NSEL):
                 found = jnp.where(chosen[b, e] == me * kblocks + w, b * NSEL + e, found)
             table[b, n + w] = found
-    part[:, entries] = jnp.zeros_like(part[:, entries])
-
-    def kv_copy(j):
-        return remote(give.at[j], pool.at[me], kv_send.at[j], kv_recv.at[me], {"kv": j})
-
-    def answer(k, _):
-        j = n - 1 - k
-        remote(ask.at[0], asked.at[j], ask_send.at[0], ask_recv.at[j], {"kv": after}).wait_recv()
-        named = asked[j]
-        for a, ref in ((0, keys), (1, values)):
-            block = jnp.zeros((KB, kv_cols), F32)
-            for w in range(kblocks):
-                mask = jnp.concatenate([named == w + 1] * (KB // 8), axis=0)
-                block = jnp.where(mask, ref[w].astype(F32), block)
-            give[j, a] = block.astype(BF16)
-        kv_copy(j).start()
-        return 0
-
-    lax.fori_loop(0, n - 1 - me, answer, 0)
-
-    def norm_each(act, act_local):
+    part[:, :, entries] = jnp.zeros_like(part[:, :, entries])
+
+    def kv_copy(g, j):
+        return remote(
+            give.at[g, j], pools[g].at[me], kv_send.at[g, j], kv_recv.at[g, me], {"kv": j}
+        )
+
+    def answer(g):
+        lanes = slice(g * HD, (g + 1) * HD)
+
+        def body(k, _):
+            j = n - 1 - k
+            if g == 0:
+                remote(
+                    ask.at[0], asked.at[j], ask_send.at[0], ask_recv.at[j], {"kv": after}
+                ).wait_recv()
+            named = asked[j]
+            for a, ref in ((0, keys), (1, values)):
+                block = jnp.zeros((KB, HD), F32)
+                for w in range(kblocks):
+                    mask = jnp.concatenate([named == w + 1] * (KB // 8), axis=0)
+                    block = jnp.where(mask, ref[w, :, lanes].astype(F32), block)
+                give[g, j, a] = block.astype(BF16)
+            kv_copy(g, j).start()
+            return 0
+
+        lax.fori_loop(0, n - 1 - me, body, 0)
+
+    def norm_each(act, act_local, ds, lower, upper):
         def body(k0, _):
-            for d in range(tp):
+            for d in ds:
                 t = (col + tp - d) % tp
                 k = (k0 + me) % per
                 dest = t * per + k
                 src = norm_parts.at[col, k] if d == 0 else norm_via.at[d, k]
 
-                @pl.when(dest == me)
+                @pl.when((dest == me) & upper)
                 def _():
                     act_local(
                         pltpu.make_async_copy(src, norm_pool.at[col, me], norm_recv.at[me])
                     )
 
-                @pl.when(dest != me)
+                @pl.when(((dest < me) & lower) | ((dest > me) & upper))
                 def _():
                     act(
                         remote(
@@ -307,32 +320,49 @@
 
         lax.fori_loop(0, per, body, 0)
 
+    def begin(c):
+        c.start()
+
+    norm_each(begin, begin, (0,), True, False)
+    for g in range(kv_heads):
+        answer(g)
     for d in range(1, tp):
         via_copy(d).wait_recv()
-    norm_each(lambda c: c.start(), lambda c: c.start())
+    norm_each(begin, begin, range(1, tp), True, False)
+    norm_each(begin, begin, range(1, tp), False, True)
+    norm_each(begin, begin, (0,), False, True)
 
     for c in own:
         c.wait()
 
-    def kv_wait(j, _):
-        remote(give.at[0], pool.at[j], kv_send.at[0], kv_recv.at[j], {"kv": after}).wait_recv()
-        return 0
-
-    lax.fori_loop(0, me, kv_wait, 0)
     span = NSEL * KB
     width = group * QB
     key_iota = lax.broadcasted_iota(jnp.int32, (KB, width), 0)
     row_iota = lax.broadcasted_iota(jnp.int32, (KB, width), 1) % QB
     logs = logsum[...].T
-    for b in range(qblocks):
-        for e in range(NSEL):
-            block = chosen[b, e]
-            owner = block // kblocks
-            slot = jnp.where(owner == me, n + block % kblocks, jnp.where(owner < me, owner, n))
-            for a in range(2):
-                sel[a, e * KB : (e + 1) * KB, :] = pool[slot, a]
-        for g in range(kv_heads):
-            lanes = slice(g * HD, (g + 1) * HD)
+
+    def back_copy(g, i):
+        return remote(
+            back.at[g, i], got.at[g, me], back_send.at[g, i], back_recv.at[g, me], {"kv": i}
+        )
+
+    for g in range(kv_heads):
+        lanes = slice(g * HD, (g + 1) * HD)
+
+        def kv_wait(j, _):
+            remote(
+                give.at[g, 0], pools[g].at[j], kv_send.at[g, 0], kv_recv.at[g, j], {"kv": after}
+            ).wait_recv()
+            return 0
+
+        lax.fori_loop(0, me, kv_wait, 0)
+        for b in range(qblocks):
+            for e in range(NSEL):
+                block = chosen[b, e]
+                owner = block // kblocks
+                slot = jnp.where(owner == me, n + block % kblocks, jnp.where(owner < me, owner, n))
+                for a in range(2):
+                    sel[a, e * KB : (e + 1) * KB] = pools[g][slot, a]
 
             def stack(ref):
                 return jnp.concatenate(
@@ -345,9 +375,9 @@
 
             q = stack(queries)
             do = stack(out_grad)
-            k_sel = sel[0, :, lanes]
+            k_sel = sel[0]
             s_buf[...] = dot(k_sel, q, ((1,), (1,)))
-            d_buf[...] = dot(sel[1, :, lanes], do, ((1,), (1,)))
+            d_buf[...] = dot(sel[1], do, ((1,), (1,)))
             log = jnp.concatenate(
                 [
                     logs[g * group + h : g * group + h + 1, b * QB : (b + 1) * QB]
@@ -371,34 +401,32 @@
                 ds_low[at, :] = (s_buf[at, :] * (d_buf[at, :] - delta)).astype(BF16)
             ds = ds_low[...]
             here = slice(b * NSEL, (b + 1) * NSEL)
-            part[0, here, :, lanes] = (dot(ds, q, ((1,), (0,))) * scale).reshape(NSEL, KB, HD)
-            part[1, here, :, lanes] = dot(p_low[...], do, ((1,), (0,))).reshape(NSEL, KB, HD)
+            part[g, 0, here] = (dot(ds, q, ((1,), (0,))) * scale).reshape(NSEL, KB, HD)
+            part[g, 1, here] = dot(p_low[...], do, ((1,), (0,))).reshape(NSEL, KB, HD)
             dq = dot(ds, k_sel, ((0,), (0,))) * scale
             for h in range(group):
                 query_grad[
                     b * QB : (b + 1) * QB, (g * group + h) * HD : (g * group + h + 1) * HD
                 ] = dq[h * QB : (h + 1) * QB]
 
-    def back_copy(i):
-        return remote(back.at[i], got.at[me], back_send.at[i], back_recv.at[me], {"kv": i})
-
-    def send_back(i, _):
-        for a in range(2):
-            total = part[a, table[0, i]]
-            for b in range(1, qblocks):
-                total = total + part[a, table[b, i]]
-            back[i, a] = total.astype(BF16)
-        back_copy(i).start()
-        return 0
-
-    lax.fori_loop(0, me, send_back, 0)
+        def send_back(i, _):
+            for a in range(2):
+                total = part[g, a, table[0, i]]
+                for b in range(1, qblocks):
+                    total = total + part[g, a, table[b, i]]
+                back[g, i, a] = total.astype(BF16)
+            back_copy(g, i).start()
+            return 0
+
+        lax.fori_loop(0, me, send_back, 0)
 
     for w in range(kblocks):
-        for a, out in ((0, key_grad), (1, value_grad)):
-            total = part[a, table[0, n + w]]
-            for b in range(1, qblocks):
-                total = total + part[a, table[b, n + w]]
-            out[w] = total
+        for g in range(kv_heads):
+            for a, out in ((0, key_grad), (1, value_grad)):
+                total = part[g, a, table[0, n + w]]
+                for b in range(1, qblocks):
+                    total = total + part[g, a, table[b, n + w]]
+                out[w, :, g * HD : (g + 1) * HD] = total
 
     def swap_copy(d):
         q = (col + d) % tp
@@ -412,70 +440,82 @@
         ).wait()
         return 0
 
-    lax.fori_loop(0, n, norm_wait, 0)
-    for d in range(1, tp):
-        swap_copy(d).start()
-
-    def add_back(j, _):
-        remote(
-            back.at[0], got.at[j], back_send.at[0], back_recv.at[j], {"kv": after}
-        ).wait_recv()
-        named = asked[j]
-        terms = [got[j, a].astype(F32) for a in range(2)]
-        for w in range(kblocks):
-            mask = jnp.concatenate([named == w + 1] * (KB // 8), axis=0)
-            for a, out in ((0, key_grad), (1, value_grad)):
-                out[w] += jnp.where(mask, terms[a], 0.0)
-        return 0
-
-    lax.fori_loop(me + 1, n, add_back, 0)
-
-    low_pool[me] = value_grad[...].reshape(tok, kv_cols).astype(BF16)
-    low = Gather(low_pool, lo_z, lo_x, lo_c, lo_recv, me, n, tp)
-    low.start()
-    low.relay()
+    lows = [
+        Gather(low_pool.at[g], lo_z.at[g], lo_x.at[g], lo_c.at[g], lo_recv.at[g], me, n, tp)
+        for g in range(kv_heads)
+    ]
+
+    for g in range(kv_heads):
+        lanes = slice(g * HD, (g + 1) * HD)
+
+        def add_back(j, _):
+            remote(
+                back.at[g, 0], got.at[g, j], back_send.at[g, 0], back_recv.at[g, j], {"kv": after}
+            ).wait_recv()
+            named = asked[j]
+            terms = [got[g, j, a].astype(F32) for a in range(2)]
+            for w in range(kblocks):
+                mask = jnp.concatenate([named == w + 1] * (KB // 8), axis=0)
+                for a, out in ((0, key_grad), (1, value_grad)):
+                    out[w, :, lanes] += jnp.where(mask, terms[a], 0.0)
+            return 0
+
+        lax.fori_loop(me + 1, n, add_back, 0)
+        low_pool[g, me] = value_grad[:, :, lanes].reshape(tok, HD).astype(BF16)
+        lows[g].start()
+        if g == 0:
+            lax.fori_loop(0, n, norm_wait, 0)
+            for d in range(1, tp):
+                swap_copy(d).start()
+
+    for low in lows:
+        low.relay()
     for d in range(1, tp):
         q = (col + tp - d) % tp
         remote(
             norm_pool.at[q], norm_pool.at[q], swap_send.at[d], swap_recv.at[d], {"tp": q}
         ).wait_recv()
-    low.finish()
-
-    row = low.row
-
-    def product(z, q):
-        a = jnp.concatenate([norm_pool[q, z * row + i] for i in range(row)], axis=1)
-        v = jnp.concatenate([low_pool[z * row + i] for i in range(row)], axis=0)
-        return dot(a, v, ((1,), (0,)))
-
-    for q in range(tp):
-        weight_grad[q * sub : (q + 1) * sub] = product(0, q)
-
-    def weigh(z, _):
+    row, zs = lows[0].row, lows[0].zs
+    for g in range(kv_heads):
+        lanes = slice(g * HD, (g + 1) * HD)
+        lows[g].finish()
+
+        def product(z, q):
+            a = jnp.concatenate([norm_pool[q, z * row + i] for i in range(row)], axis=1)
+            v = jnp.concatenate([low_pool[g, z * row + i] for i in range(row)], axis=0)
+            return dot(a, v, ((1,), (0,)))
+
         for q in range(tp):
-            weight_grad[q * sub : (q + 1) * sub] += product(z, q)
-        return 0
-
-    lax.fori_loop(1, low.zs, weigh, 0)
-
-    low.drain()
+            weight_grad[q * sub : (q + 1) * sub, lanes] = product(0, q)
+
+        def weigh(z, _):
+            for q in range(tp):
+                weight_grad[q * sub : (q + 1) * sub, lanes] += product(z, q)
+            return 0
+
+        lax.fori_loop(1, zs, weigh, 0)
+
+    for low in lows:
+        low.drain()
 
     def drain_early(i, _):
         ask_copy(i).wait_send()
-        back_copy(i).wait_send()
+        for g in range(kv_heads):
+            back_copy(g, i).wait_send()
         return 0
 
     lax.fori_loop(0, me, drain_early, 0)
 
     def drain_late(j, _):
-        kv_copy(j).wait_send()
+        for g in range(kv_heads):
+            kv_copy(g, j).wait_send()
         return 0
 
     lax.fori_loop(me + 1, n, drain_late, 0)
     for d in range(1, tp):
         via_copy(d).wait_send()
         swap_copy(d).wait_send()
-    norm_each(lambda c: c.wait_send(), lambda c: None)
+    norm_each(lambda c: c.wait_send(), lambda c: None, range(tp), True, True)
 
 
 def local(n, tp, queries, keys, values, logsum, out_grad, normed_input, chosen):
@@ -503,41 +543,41 @@
         in_specs=[pl.BlockSpec(memory_space=pltpu.SMEM)] + [vmem] * 6,
         out_specs=(vmem,) * 4,
         scratch_shapes=[
-            pltpu.VMEM((n + kblocks, 2, KB, kv_cols), BF16),
-            pltpu.VMEM((n, 8, kv_cols), jnp.int32),
-            pltpu.VMEM((n, 8, kv_cols), jnp.int32),
-            pltpu.VMEM((n, 2, KB, kv_cols), BF16),
-            pltpu.VMEM((n, tok, kv_cols), BF16),
+            pltpu.VMEM((n, 8, HD), jnp.int32),
+            pltpu.VMEM((n, 8, HD), jnp.int32),
+            pltpu.VMEM((kv_heads, n, 2, KB, HD), BF16),
+            pltpu.VMEM((kv_heads, n, tok, HD), BF16),
             pltpu.VMEM((tp, per, rows // tp, tok), BF16),
             pltpu.VMEM((tp, per, rows // tp, tok), BF16),
             pltpu.VMEM((tp, n, rows // tp, tok), BF16),
-            pltpu.VMEM((2, span, kv_cols), BF16),
+            pltpu.VMEM((2, span, HD), BF16),
             pltpu.VMEM((span, width), F32),
             pltpu.VMEM((span, width), F32),
             pltpu.VMEM((span, width), BF16),
             pltpu.VMEM((span, width), BF16),
-            pltpu.VMEM((2, entries + 1, KB, kv_cols), F32),
-            pltpu.VMEM((n, 2, KB, kv_cols), BF16),
-            pltpu.VMEM((n, 2, KB, kv_cols), BF16),
+            pltpu.VMEM((kv_heads, 2, entries + 1, KB, HD), F32),
+            pltpu.VMEM((kv_heads, n, 2, KB, HD), BF16),
+            pltpu.VMEM((kv_heads, n, 2, KB, HD), BF16),
             pltpu.SMEM((qblocks, n + kblocks), jnp.int32),
-            dma((kblocks, 2)),
+            dma((kv_heads, kblocks, 2)),
             dma((n,)),
             dma((n,)),
-            dma((n,)),
-            dma((n,)),
-            dma((n,)),
-            dma((n,)),
+            dma((kv_heads, n)),
+            dma((kv_heads, n)),
+            dma((kv_heads, n)),
+            dma((kv_heads, n)),
             dma((tp,)),
             dma((tp,)),
             dma((tp, per)),
             dma((n,)),
             dma((tp,)),
             dma((tp,)),
-            dma((zs,)),
-            dma((zs, tp)),
-            dma((zs, tp)),
-            dma((n,)),
-        ],
+            dma((kv_heads, zs)),
+            dma((kv_heads, zs, tp)),
+            dma((kv_heads, zs, tp)),
+            dma((kv_heads, n)),
+        ]
+        + [pltpu.VMEM((n + kblocks, 2, KB, HD), BF16)] * kv_heads,
         compiler_params=pltpu.CompilerParams(
             collective_id=0, has_side_effects=True, vmem_limit_bytes=60 * 1024 * 1024
         ),

time: 65.7 us -> 66 us (level)
  the two profiles are of different devices: /device:TPU:23 before, /device:TPU:0 now
where the time goes in v3:
time: 66 us; the launch traced here: 65.2 us
  Pallas kernels  58.8 us (89%)
  local copies, waits for them, and re-layouts  5.79 us (9%)
  between operations  0.66 us (1%)
    pallas_call x1, Pallas kernels, local(): pl.pallas_call(functools.partial(kernel, n, tp), out_shape=(jax.ShapeDtyp...  58.8 us
    unnamed x11, local copies, waits for them, and re-layouts  5.79 us

profile of v3, /device:TPU:0, one launch (start us, length us, event | category | flops | bytes accessed | tf_op | source)
XLA Modules:
  0.0 65.2 jit_solution(4959615409566015649)
XLA Ops:
  0.6 1.4 %copy.11.logsum = f32[128,16]{1,0:T(8,128)} copy(f32[128,16]{0,1:T(8,128)} %param.10) | data formatting | bytes 16384 | tf_op args[3]
  2.1 58.8 %attention_back.1 = (f32[128,2048]{1,0:T(8,128)}, f32[4,32,256]{2,1,0:T(8,128)}, f32[4,32,256]{2,1,0:T(8,128)}, f32[256,256]{1,0:T(8,128)}) custom-call(s32[2,16]{1,0:T(2,128)} %chosen.1, bf16[128,2048]{1,0:T(8,128)(2,1)} %queries.1, bf16[4,32,256]{2,1,0:T(8,128)(2,1)} %bitcast.6, bf16[4,32,256]{2,1,0:T(8,128)(2,1)} %bitcast.7, f32[128,16]{1,0:T(8,128)} %copy.11.logsum, ...), custom_call_target="tpu_custom_call" | custom-call | tf_op jit(solution)/shard_map/attention_back/pallas_call | solution.py:535
  60.8 0.0 copy-start.2
  60.9 0.0 copy-start.1
  60.9 2.3 %copy.16 = f32[128,2048]{1,0:T(8,128)} copy(f32[128,2048]{1,0:T(8,128)} %get-tuple-element.16) | data formatting | bytes 2097152
  63.2 0.0 copy-done.2
  63.2 0.0 copy-start
  63.2 0.7 %copy.17 = f32[128,256]{1,0:T(8,128)} copy(f32[128,256]{1,0:T(8,128)S(1)} %bitcast.5) | data formatting | bytes 262144
  63.9 0.0 copy-done.1
  63.9 0.7 %copy.18 = f32[128,256]{1,0:T(8,128)} copy(f32[128,256]{1,0:T(8,128)S(1)} %bitcast.4) | data formatting | bytes 262144
  64.5 0.0 copy-done
  64.5 0.7 %copy.19 = f32[256,256]{1,0:T(8,128)} copy(f32[256,256]{1,0:T(8,128)S(1)} %copy-done) | data formatting | bytes 524288
Async XLA Ops:
  60.8 2.4 %copy-start.2 = (f32[4,32,256]{2,1,0:T(8,128)S(1)}, f32[4,32,256]{2,1,0:T(8,128)}, u32[]{:S(2)}) copy-start(f32[4,32,256]{2,1,0:T(8,128)} %get-tuple-element.9) | copy-start | bytes 393220
  60.9 3.0 %copy-start.1 = (f32[4,32,256]{2,1,0:T(8,128)S(1)}, f32[4,32,256]{2,1,0:T(8,128)}, u32[]{:S(2)}) copy-start(f32[4,32,256]{2,1,0:T(8,128)} %get-tuple-element.10) | copy-start | bytes 393220
  63.2 1.3 %copy-start = (f32[256,256]{1,0:T(8,128)S(1)}, f32[256,256]{1,0:T(8,128)}, u32[]{:S(2)}) copy-start(f32[256,256]{1,0:T(8,128)} %get-tuple-element.19) | copy-start | bytes 786436
